TPU v7x, 32 devices: a whole 2x2x4 slice. The times are simulated.
32 devices in a mesh: grp: 2 (over y), sp: 4 (over z), tp: 4 (over x, core).
Axes of the slice: x: 2, y: 2, z: 4, core: 2. Of those that a mesh axis runs over, the one named last changes fastest.
Arguments:
- query_first: bfloat16 [1536, 512], P(('grp', 'sp'), 'tp'), parts along dimension 0, may hold values from -172 to 172
- key_first: bfloat16 [1536, 512], P(('grp', 'sp'), 'tp'), parts along dimension 0, may hold values from -7.8 to 7.8
- query_second: bfloat16 [1536, 1024], P(('grp', 'sp'), 'tp'), parts along dimension 0, may hold values from -172 to 172
- key_second: bfloat16 [1536, 1024], P(('grp', 'sp'), 'tp'), parts along dimension 0, may hold values from -7.8 to 7.8
- values: bfloat16 [1536, 2, 512], P(('grp', 'sp'), None, 'tp'), parts along dimension 0, may hold values from -6 to 6
- lambdas: float32 [2, 4], P(None, 'tp'), may hold values from 0.3 to 0.8
- residual: bfloat16 [1536, 2048], P(('grp', 'sp'), 'tp'), parts along dimension 0, may hold values from -130 to 130
- norm_gain: bfloat16 [2048], P('tp'), may hold values from 0.099609375 to 1.8984375
- out_weight: bfloat16 [2, 512, 2048], P(None, 'tp'), may hold values from -0.1875 to 0.1875
- gate_weight: bfloat16 [2048, 5632], P('sp', 'tp'), may hold values from -0.125 to 0.125
- up_weight: bfloat16 [2048, 5632], P('sp', 'tp'), may hold values from -0.125 to 0.125
- down_weight: bfloat16 [5632, 2048], P('tp', 'sp'), may hold values from -0.078125 to 0.078125
Outputs:
- layer_out: bfloat16 [1536, 2048], P(('grp', 'sp'), 'tp'), parts along dimension 0
There are 2 independent parts, one for each index of `grp`. A program takes and returns all parts, laid end to end along the dimension named above; an argument that names none is the same for every part. Nothing has to cross between parts.
All inputs are finite; a program needn't handle non-finite values.
Results may differ from a plain program's by a relative error of at most 0.0065.
Values may be sent and summed in bfloat16 or wider, within the bound.
A program may use at most 128 MiB of HBM per device.

v0:
```python
import jax
import jax.numpy as jnp
from jax import lax
from jax.sharding import PartitionSpec as P

D = 2048


def per_device(
    query_first,
    key_first,
    query_second,
    key_second,
    values,
    lambdas,
    residual,
    norm_gain,
    out_weight,
    gate_weight,
    up_weight,
    down_weight,
):
    tok_rows = query_first.shape[0]
    heads_here = lambdas.shape[1]
    width_first = query_first.shape[1] // (2 * heads_here)
    width_second = query_second.shape[1] // (2 * heads_here)
    value_size = values.shape[2] // heads_here
    offset = lax.axis_index("sp") * tok_rows
    query_pos = offset + lax.broadcasted_iota(jnp.int32, (tok_rows, 1), 0)
    query_groups = (
        query_first.reshape(tok_rows, heads_here, 2, width_first),
        query_second.reshape(tok_rows, heads_here, 2, width_second),
    )
    key_widths = (width_first, width_second)
    start_state = (
        jnp.full((heads_here, 2, tok_rows, 1), -1e30, jnp.float32),
        jnp.zeros((heads_here, 2, tok_rows, 1), jnp.float32),
        jnp.zeros((heads_here, 2, tok_rows, value_size), jnp.float32),
    )
    states = (start_state, start_state)
    pieces = (
        lax.all_gather(key_first, "sp", axis=0, tiled=True),
        lax.all_gather(key_second, "sp", axis=0, tiled=True),
        lax.all_gather(values, "sp", axis=0, tiled=True),
    )
    piece_rows = pieces[0].shape[0]
    key_pos = lax.broadcasted_iota(jnp.int32, (1, piece_rows), 1)
    allowed = key_pos <= query_pos
    value_rows = pieces[2].reshape(piece_rows, 2, heads_here, value_size)
    results = []
    for group_idx in range(2):
        key_width = key_widths[group_idx]
        key_part = pieces[group_idx].reshape(piece_rows, heads_here, 2, key_width)
        scores = jnp.einsum(
            "qhmd,khmd->hmqk", query_groups[group_idx], key_part, preferred_element_type=jnp.float32
        ) * key_width ** (-0.5)
        scores = jnp.where(allowed, scores, -1e30)
        running, totals, weighted = states[group_idx]
        new_peak = jnp.maximum(running, jnp.max(scores, axis=-1, keepdims=True))
        weights = jnp.where(allowed, jnp.exp(scores - new_peak), 0.0)
        totals = jnp.sum(weights, axis=-1, keepdims=True)
        weighted = jnp.einsum(
            "hmqk,khe->hmqe",
            weights.astype(jnp.bfloat16),
            value_rows[:, group_idx],
            preferred_element_type=jnp.float32,
        )
        results.append((new_peak, totals, weighted))
    states = (results[0], results[1])
    map_out = jnp.stack([states[0][2] / states[0][1], states[1][2] / states[1][1]])
    differ = map_out[:, :, 0] - lambdas[:, :, None, None] * map_out[:, :, 1]
    head_scale = lax.rsqrt(jnp.mean(differ * differ, axis=-1, keepdims=True) + 1e-06)
    attended = (0.8 * differ * head_scale).astype(jnp.bfloat16)
    projection = out_weight.reshape(2, heads_here, value_size, out_weight.shape[2])
    mixed_part = jnp.einsum(
        "ghqe,gher->qr", attended, projection, preferred_element_type=jnp.float32
    )
    mixed = lax.psum_scatter(
        mixed_part.astype(jnp.bfloat16), "tp", scatter_dimension=1, tiled=True
    ).astype(jnp.float32)
    stream = residual.astype(jnp.float32) + mixed
    squares = lax.psum(jnp.sum(stream * stream, axis=1), "tp")
    row_scale = lax.rsqrt(squares[:, None] / D + 1e-06)
    normed = (stream * row_scale * norm_gain.astype(jnp.float32)).astype(jnp.bfloat16)
    full_rows = lax.all_gather(normed, "tp", axis=1, tiled=True)
    pieces = (
        lax.all_gather(gate_weight, "sp", axis=0, tiled=True),
        lax.all_gather(up_weight, "sp", axis=0, tiled=True),
    )
    gate = jnp.dot(full_rows, pieces[0], preferred_element_type=jnp.float32)
    up_part = jnp.dot(full_rows, pieces[1], preferred_element_type=jnp.float32)
    hidden = (jax.nn.silu(gate) * up_part).astype(jnp.bfloat16)
    partial_out = jnp.dot(
        hidden,
        lax.all_gather(down_weight, "sp", axis=1, tiled=True),
        preferred_element_type=jnp.float32,
    )
    ffn = lax.psum_scatter(
        partial_out.astype(jnp.bfloat16), "tp", scatter_dimension=1, tiled=True
    ).astype(jnp.float32)
    return (stream + 0.5 * ffn).astype(jnp.bfloat16)


def solution(mesh):
    return jax.shard_map(
        per_device,
        mesh=mesh,
        in_specs=(
            P(("grp", "sp"), "tp"),
            P(("grp", "sp"), "tp"),
            P(("grp", "sp"), "tp"),
            P(("grp", "sp"), "tp"),
            P(("grp", "sp"), None, "tp"),
            P(None, "tp"),
            P(("grp", "sp"), "tp"),
            P("tp"),
            P(None, "tp", None),
            P("sp", "tp"),
            P("sp", "tp"),
            P("tp", "sp"),
        ),
        out_specs=P(("grp", "sp"), "tp"),
        check_vma=False,
    )
```

profile of v0, /device:TPU:0, one launch (start us, length us, event | category | flops | bytes accessed | tf_op | source)
XLA Modules:
  0.0 419.4 jit_solution(9682786560967322755)
XLA Ops:
  7.4 0.0 copy-start
  7.4 0.0 copy-start.6
  7.4 0.0 copy-start.5
  7.4 0.0 copy-start.4
  7.4 0.0 reduce-scatter.3.cloned.1.call-start
  7.4 0.1 iota_compare_fusion
  7.6 16.6 %all_gather.23 = bf16[768,256]{1,0:T(8,128)(2,1)S(1)} all-gather(bf16[192,256]{1,0:T(8,128)(2,1)} %param.15), channel_id=1, replica_groups=mesh['grp'=2,'sp'=4,'tp'=4] {'sp'}, dimensions={0}, use_global_device_ids=true | all-gather | bytes 491520 | tf_op jit(solution)/shard_map/all_gather | solution.py:43
  24.2 0.0 copy-start.3
  24.2 0.2 copy.28
  24.4 0.0 copy-done.6
  24.4 14.4 %all_gather.21 = bf16[768,128]{1,0:T(8,128)(2,1)S(1)} all-gather(bf16[192,128]{1,0:T(8,128)(2,1)S(1)} %copy-done.6), channel_id=1, replica_groups=mesh['grp'=2,'sp'=4,'tp'=4] {'sp'}, dimensions={0}, use_global_device_ids=true | all-gather | bytes 245760 | tf_op jit(solution)/shard_map/all_gather | solution.py:42
  38.8 0.1 copy.26
  38.9 0.0 copy-done.5
  38.9 0.1 copy.25
  39.0 0.0 copy-done.4
  39.1 14.8 %all_gather.22 = bf16[768,2,128]{2,0,1:T(8,128)(2,1)S(1)} all-gather(bf16[192,2,128]{2,0,1:T(8,128)(2,1)S(1)} %copy.27), channel_id=1, replica_groups=mesh['grp'=2,'sp'=4,'tp'=4] {'sp'}, dimensions={0}, use_global_device_ids=true | all-gather | bytes 491520 | tf_op jit(solution)/shard_map/all_gather | solution.py:44
  53.8 0.0 copy-done.3
  53.8 0.5 fusion.34
  54.3 0.5 fusion.35
  54.8 0.7 fusion.6
  55.5 0.4 fusion.5
  55.9 0.0 copy-start.7
  55.9 0.4 fusion.4
  56.4 0.2 copy-done.7
  56.6 0.2 fusion.21
  56.8 0.0 copy-done
  56.8 1.3 fusion
  58.2 0.0 reduce-scatter.3.cloned.1.call-update
  58.2 0.0 all-gather.4.cloned.1.call-start
  58.3 0.5 all-gather.4.cloned.1.call-update
  58.8 0.0 copy-start.8
  58.8 0.0 copy-start.1
  58.8 0.0 all-gather.6.cloned.1.call-start
  58.9 0.5 all-gather.6.cloned.1.call-update
  59.4 0.0 all-gather.8.cloned.1.call-start
  59.4 0.5 all-gather.8.cloned.1.call-update
  60.0 0.0 reduce-scatter.5.cloned.1.call-start
  60.0 0.0 copy-done.8
  60.0 22.8 %reduce-scatter.3.cloned.1.call-done = bf16[192,512]{1,0:T(8,128)(2,1)} async-done(((bf16[192,2048]{1,0:T(8,128)(2,1)}), bf16[192,512]{1,0:T(8,128)(2,1)}) %reduce-scatter.3.cloned.1.call-update) | async-done | bytes 196624 | tf_op jit(solution)/shard_map/reduce_scatter | solution.py:78
  82.8 0.0 copy-done.1
  82.8 1.1 multiply_reduce_fusion
  83.9 6.1 %psum.7 = f32[192]{0:T(256)S(1)} all-reduce(f32[192]{0:T(256)S(1)} %multiply_reduce_fusion), channel_id=1, replica_groups=mesh['grp'=2,'sp'=4,'tp'=4] {'tp'}, use_global_device_ids=true, to_apply=%region_7.8 | all-reduce | flops 192 | bytes 1536 | tf_op jit(solution)/shard_map/psum | solution.py:82
  90.0 1.0 multiply_convert_fusion
  91.0 8.4 %all_gather.24 = bf16[192,2048]{1,0:T(8,128)(2,1)S(1)} all-gather(bf16[192,512]{1,0:T(8,128)(2,1)S(1)} %multiply_convert_fusion), channel_id=1, replica_groups=mesh['grp'=2,'sp'=4,'tp'=4] {'tp'}, dimensions={1}, use_global_device_ids=true | all-gather | bytes 983040 | tf_op jit(solution)/shard_map/all_gather | solution.py:85
  99.4 68.7 %all-gather.4.cloned.1.call-done = bf16[2048,1408]{1,0:T(8,128)(2,1)} async-done(((bf16[512,1408]{1,0:T(8,128)(2,1)}), bf16[2048,1408]{1,0:T(8,128)(2,1)}) %all-gather.4.cloned.1.call-update) | async-done | bytes 5767184 | tf_op jit(solution)/shard_map/all_gather | solution.py:87
  168.1 4.0 fusion.36
  172.1 0.0 copy-start.2
  172.1 102.2 %all-gather.6.cloned.1.call-done = bf16[2048,1408]{1,0:T(8,128)(2,1)} async-done(((bf16[512,1408]{1,0:T(8,128)(2,1)}), bf16[2048,1408]{1,0:T(8,128)(2,1)}) %all-gather.6.cloned.1.call-update) | async-done | bytes 5767184 | tf_op jit(solution)/shard_map/all_gather | solution.py:88
  274.4 106.3 %all-gather.8.cloned.1.call-done = bf16[1408,2048]{1,0:T(8,128)(2,1)} async-done(((bf16[1408,512]{1,0:T(8,128)(2,1)}), bf16[1408,2048]{1,0:T(8,128)(2,1)}) %all-gather.8.cloned.1.call-update) | async-done | bytes 5767184 | tf_op jit(solution)/shard_map/all_gather | solution.py:95
  380.6 7.9 %convolution_convert_fusion = bf16[192,2048]{1,0:T(8,128)(2,1)} fusion(bf16[1408,2048]{1,0:T(8,128)(2,1)} %all-gather.8.cloned.1.call-done, bf16[192,2048]{1,0:T(8,128)(2,1)S(1)} %all_gather.24, bf16[2048,1408]{1,0:T(8,128)(2,1)} %all-gather.6.cloned.1.call-done, f32[192,1408]{1,0:T(8,128)S(1)} %fusion.36), kind=kOutput, calls=%fused_computation.4 | convolution fusion | flops 2216607744 | bytes 14188544 | tf_op jit(solution)/shard_map/dot_general | solution.py:93
  388.5 0.0 reduce-scatter.5.cloned.1.call-update
  388.5 21.6 %reduce-scatter.5.cloned.1.call-done = bf16[192,512]{1,0:T(8,128)(2,1)} async-done(((bf16[192,2048]{1,0:T(8,128)(2,1)}), bf16[192,512]{1,0:T(8,128)(2,1)}) %reduce-scatter.5.cloned.1.call-update) | async-done | bytes 196624 | tf_op jit(solution)/shard_map/reduce_scatter | solution.py:98
  410.2 0.0 copy-done.2
  410.2 1.7 add_convert_fusion
  (6 shorter events, 0.0 us)
Async XLA Ops:
  7.4 49.5 %copy-start = (bf16[2,128,2048]{2,1,0:T(8,128)(2,1)S(1)}, bf16[2,128,2048]{2,1,0:T(8,128)(2,1)}, u32[]{:S(2)}) copy-start(bf16[2,128,2048]{2,1,0:T(8,128)(2,1)} %param.20) | copy-start | bytes 3145732
  7.4 17.0 %copy-start.6 = (bf16[192,128]{1,0:T(8,128)(2,1)S(1)}, bf16[192,128]{1,0:T(8,128)(2,1)}, u32[]{:S(2)}) copy-start(bf16[192,128]{1,0:T(8,128)(2,1)} %param.13) | copy-start | bytes 147460
  7.4 31.5 %copy-start.5 = (bf16[192,128]{1,0:T(8,128)(2,1)S(1)}, bf16[192,128]{1,0:T(8,128)(2,1)}, u32[]{:S(2)}) copy-start(bf16[192,128]{1,0:T(8,128)(2,1)} %param.12) | copy-start | bytes 147460
  7.4 31.7 %copy-start.4 = (bf16[192,2,128]{2,1,0:T(2,128)(2,1)S(1)}, bf16[192,2,128]{2,1,0:T(2,128)(2,1)}, u32[]{:S(2)}) copy-start(bf16[192,2,128]{2,1,0:T(2,128)(2,1)} %param.16) | copy-start | bytes 294916
  7.4 75.4 %reduce-scatter.3.cloned.1.call-start = ((), (), s32[]{:S(2)}) async-start(), calls=%async_computation.2 | async-start | bytes 983040 | tf_op jit(solution)/shard_map/reduce_scatter | solution.py:78
  24.2 29.6 %copy-start.3 = (bf16[192,256]{1,0:T(8,128)(2,1)S(1)}, bf16[192,256]{1,0:T(8,128)(2,1)}, u32[]{:S(2)}) copy-start(bf16[192,256]{1,0:T(8,128)(2,1)} %param.14) | copy-start | bytes 294916
  55.9 0.7 copy-start.7
  58.2 109.9 %all-gather.4.cloned.1.call-start = ((), (), s32[]{:S(2)}) async-start(), calls=%async_computation.3 | async-start | bytes 7208960 | tf_op jit(solution)/shard_map/all_gather | solution.py:87
  58.8 1.2 copy-start.8
  58.8 24.0 %copy-start.1 = (bf16[192,512]{1,0:T(8,128)(2,1)S(1)}, bf16[192,512]{1,0:T(8,128)(2,1)}, u32[]{:S(2)}) copy-start(bf16[192,512]{1,0:T(8,128)(2,1)} %param.18) | copy-start | bytes 589828
  58.8 215.6 %all-gather.6.cloned.1.call-start = ((), (), s32[]{:S(2)}) async-start(), calls=%async_computation.4 | async-start | bytes 7208960 | tf_op jit(solution)/shard_map/all_gather | solution.py:88
  59.4 321.3 %all-gather.8.cloned.1.call-start = ((), (), s32[]{:S(2)}) async-start(), calls=%async_computation.5 | async-start | bytes 7208960 | tf_op jit(solution)/shard_map/all_gather | solution.py:95
  60.0 350.2 %reduce-scatter.5.cloned.1.call-start = ((), (), s32[]{:S(2)}) async-start(), calls=%async_computation.6 | async-start | bytes 983040 | tf_op jit(solution)/shard_map/reduce_scatter | solution.py:98
  172.1 238.0 %copy-start.2 = (bf16[192,512]{1,0:T(8,128)(2,1)S(1)}, bf16[192,512]{1,0:T(8,128)(2,1)}, u32[]{:S(2)}) copy-start(bf16[192,512]{1,0:T(8,128)(2,1)} %reduce-scatter.3.cloned.1.call-done) | copy-start | bytes 589828
Sparse Core Ops, SparseCore 0:
  58.3 24.4 reduce-scatter.2
  388.7 21.4 reduce-scatter.4
Sparse Core Ops, SparseCore 1:
  60.3 107.8 all-gather.3
  169.5 104.8 all-gather.5
  275.8 104.8 all-gather.7
where the time goes:
time: 420 us; the launch traced here: 419 us
  waiting for transfers between devices  323 us (77%)
  blocking collectives  60.2 us (14%)
  between operations  15.2 us (4%)
  matrix products  15.1 us (4%)
  other arithmetic  4.87 us (1%)
    all_gather x1, waiting for transfers between devices, per_device(): lax.all_gather(down_weight, 'sp', axis=1, tiled=True)  106 us
    all_gather x1, waiting for transfers between devices, per_device(): lax.all_gather(up_weight, 'sp', axis=0, tiled=True)  102 us
    all_gather x1, waiting for transfers between devices, per_device(): lax.all_gather(gate_weight, 'sp', axis=0, tiled=True)  68.7 us
    reduce_scatter x1, waiting for transfers between devices, per_device(): lax.psum_scatter(mixed_part.astype(jnp.bfloat16), 'tp', scatter_dimension...  22.8 us
    reduce_scatter x1, waiting for transfers between devices, per_device(): lax.psum_scatter(partial_out.astype(jnp.bfloat16), 'tp', scatter_dimensio...  21.6 us
    all_gather x1, blocking collectives, per_device(): lax.all_gather(key_second, 'sp', axis=0, tiled=True)  16.6 us
    all_gather x1, blocking collectives, per_device(): lax.all_gather(values, 'sp', axis=0, tiled=True)  14.8 us
    all_gather x1, blocking collectives, per_device(): lax.all_gather(key_first, 'sp', axis=0, tiled=True)  14.4 us
  transfers between devices with their start and end apart: 5, of which 5 were waited for; matrix products, arithmetic and copies ran while one was open for 1% of the time, Pallas kernels for 0%

commit v1 on v0

--- a/solution.py
+++ b/solution.py
@@ -4,6 +4,25 @@
 from jax.sharding import PartitionSpec as P
 
 D = 2048
+
+
+def gather_around(x, axis, dim):
+    size, here, rows = (lax.axis_size(axis), lax.axis_index(axis), x.shape[dim])
+    forward = [(i, (i + 1) % size) for i in range(size)]
+    downward = [(i, (i - 1) % size) for i in range(size)]
+    out = jnp.zeros((*x.shape[:dim], size * rows, *x.shape[dim + 1 :]), x.dtype)
+    out = lax.dynamic_update_slice_in_dim(out, x, here * rows, axis=dim)
+    from_left = from_right = x
+    halfway = size // 2
+    for turn in range(1, halfway + 1):
+        from_left = lax.ppermute(from_left, axis, forward)
+        out = lax.dynamic_update_slice_in_dim(out, from_left, (here - turn) % size * rows, axis=dim)
+        if turn < size - halfway:
+            from_right = lax.ppermute(from_right, axis, downward)
+            out = lax.dynamic_update_slice_in_dim(
+                out, from_right, (here + turn) % size * rows, axis=dim
+            )
+    return out
 
 
 def per_device(
@@ -91,9 +110,7 @@
     up_part = jnp.dot(full_rows, pieces[1], preferred_element_type=jnp.float32)
     hidden = (jax.nn.silu(gate) * up_part).astype(jnp.bfloat16)
     partial_out = jnp.dot(
-        hidden,
-        lax.all_gather(down_weight, "sp", axis=1, tiled=True),
-        preferred_element_type=jnp.float32,
+        hidden, gather_around(down_weight, "sp", 1), preferred_element_type=jnp.float32
     )
     ffn = lax.psum_scatter(
         partial_out.astype(jnp.bfloat16), "tp", scatter_dimension=1, tiled=True

time: 420 us -> 387 us (0.921)
  waiting for transfers between devices: 323 us -> 227 us
  starting transfers between devices: 0.2 us -> 49.7 us
  local copies, waits for them, and re-layouts: 0.68 us -> 13.1 us
    all_gather x1 -> x0, waiting for transfers between devices: 106 us -> none  [per_device(): lax.all_gather(down_weight, 'sp', axis=1, tiled=True)]
    ppermute x0 -> x3, waiting for transfers between devices: none -> 95.6 us  [the longest x2 65.5 us: gather_around(): from_left = lax.ppermute(from_left, axis, forward)]
    all_gather x1, waiting for transfers between devices: 68.7 us -> 7.25 us  [per_device(): lax.all_gather(gate_weight, 'sp', axis=0, tiled=True)]
    ppermute x0 -> x3, starting transfers between devices: none -> 49.6 us  [the longest x2 47.5 us: gather_around(): from_left = lax.ppermute(from_left, axis, forward)]
    reduce_scatter x1, waiting for transfers between devices: 22.8 us -> 0.01 us  [per_device(): lax.psum_scatter(mixed_part.astype(jnp.bfloat16), 'tp', scatter_dimension...]
    dynamic_update_slice x0 -> x4, local copies, waits for them, and re-layouts: none -> 9.13 us  [the longest x2 5.28 us: gather_around(): lax.dynamic_update_slice_in_dim(out, from_left, (here - turn) % size * ro...]
  transfers between devices with their start and end apart: 5 -> 7, of which waited for: 5 -> 6; matrix products, arithmetic and copies ran while one was open for 1% -> 5% of each run, Pallas kernels for 0% -> 0%
where the time goes in v1:
time: 387 us
  waiting for transfers between devices  227 us (59%)
  blocking collectives  60.4 us (16%)
  starting transfers between devices  49.7 us (13%)
  matrix products  16.4 us (4%)
  between operations  15 us (4%)
  local copies, waits for them, and re-layouts  13.1 us (3%)
  other arithmetic  4.87 us (1%)
    all_gather x1, waiting for transfers between devices, per_device(): lax.all_gather(up_weight, 'sp', axis=0, tiled=True)  102 us
    ppermute x2, waiting for transfers between devices, gather_around(): from_left = lax.ppermute(from_left, axis, forward)  65.5 us
    ppermute x2, starting transfers between devices, gather_around(): from_left = lax.ppermute(from_left, axis, forward)  47.5 us
    ppermute x1, waiting for transfers between devices, gather_around(): from_right = lax.ppermute(from_right, axis, downward)  30.1 us
    reduce_scatter x1, waiting for transfers between devices, per_device(): lax.psum_scatter(partial_out.astype(jnp.bfloat16), 'tp', scatter_dimensio...  21.6 us
    all_gather x1, blocking collectives, per_device(): lax.all_gather(key_second, 'sp', axis=0, tiled=True)  16.6 us
    all_gather x1, blocking collectives, per_device(): lax.all_gather(values, 'sp', axis=0, tiled=True)  14.8 us
    all_gather x1, blocking collectives, per_device(): lax.all_gather(key_first, 'sp', axis=0, tiled=True)  14.4 us
  transfers between devices with their start and end apart: 7, of which 6 were waited for; matrix products, arithmetic and copies ran while one was open for 5% of the time, Pallas kernels for 0%

profile of v1, /device:TPU:0, one launch (start us, length us, event | category | flops | bytes accessed | tf_op | source)
XLA Modules:
  0.0 386.8 jit_solution(16229555358143967344)
XLA Ops:
  7.4 0.0 copy-start
  7.4 0.0 copy-start.7
  7.4 0.0 copy-start.6
  7.4 0.0 copy-start.5
  7.4 0.0 reduce-scatter.3.cloned.1.call-start
  7.4 0.1 iota_compare_fusion
  7.6 16.6 %all_gather.20 = bf16[768,256]{1,0:T(8,128)(2,1)S(1)} all-gather(bf16[192,256]{1,0:T(8,128)(2,1)} %param.15), channel_id=1, replica_groups=mesh['grp'=2,'sp'=4,'tp'=4] {'sp'}, dimensions={0}, use_global_device_ids=true | all-gather | bytes 491520 | tf_op jit(solution)/shard_map/all_gather | solution.py:62
  24.2 0.0 copy-start.4
  24.2 0.2 copy.28
  24.4 0.0 copy-done.7
  24.4 14.4 %all_gather.18 = bf16[768,128]{1,0:T(8,128)(2,1)S(1)} all-gather(bf16[192,128]{1,0:T(8,128)(2,1)S(1)} %copy-done.7), channel_id=1, replica_groups=mesh['grp'=2,'sp'=4,'tp'=4] {'sp'}, dimensions={0}, use_global_device_ids=true | all-gather | bytes 245760 | tf_op jit(solution)/shard_map/all_gather | solution.py:61
  38.8 0.1 copy.26
  38.9 0.0 copy-done.6
  38.9 0.1 copy.25
  39.0 0.0 copy-done.5
  39.1 14.8 %all_gather.19 = bf16[768,2,128]{2,0,1:T(8,128)(2,1)S(1)} all-gather(bf16[192,2,128]{2,0,1:T(8,128)(2,1)S(1)} %copy.27), channel_id=1, replica_groups=mesh['grp'=2,'sp'=4,'tp'=4] {'sp'}, dimensions={0}, use_global_device_ids=true | all-gather | bytes 491520 | tf_op jit(solution)/shard_map/all_gather | solution.py:63
  53.8 0.0 copy-done.4
  53.8 0.5 fusion.34
  54.3 0.5 fusion.35
  54.8 0.7 fusion.6
  55.5 0.4 fusion.4
  55.9 0.0 copy-start.8
  55.9 0.4 fusion.5
  56.4 0.2 copy-done.8
  56.6 0.2 fusion.21
  56.8 0.0 copy-done
  56.8 1.3 fusion
  58.2 0.0 reduce-scatter.3.cloned.1.call-update
  58.2 0.0 copy-start.3
  58.2 0.0 copy-start.9
  58.2 0.0 all-gather.3.cloned.1.call-start
  58.3 0.5 all-gather.3.cloned.1.call-update
  58.8 0.0 all-gather.5.cloned.1.call-start
  58.9 0.5 all-gather.5.cloned.1.call-update
  59.4 0.0 reduce-scatter.5.cloned.1.call-start
  59.4 0.1 copy-done.3
  59.6 2.0 collective-permute-start
  61.5 2.1 collective-permute-start.1
  63.6 0.0 copy-done.9
  63.6 3.2 broadcast_in_dim.34
  66.8 1.2 constant_dynamic-update-slice_fusion.3
  68.0 49.0 %collective-permute-done = bf16[1408,512]{1,0:T(8,128)(2,1)} collective-permute-done((bf16[1408,512]{1,0:T(8,128)(2,1)S(1)}, bf16[1408,512]{1,0:T(8,128)(2,1)}, u32[]{:S(2)}, u32[]{:S(2)}) %collective-permute-start) | collective-permute-done | bytes 1441824 | tf_op jit(solution)/shard_map/ppermute | solution.py:18
  117.0 45.5 %collective-permute-start.2 = (bf16[1408,512]{1,0:T(8,128)(2,1)}, bf16[1408,512]{1,0:T(8,128)(2,1)}, u32[]{:S(2)}, u32[]{:S(2)}) collective-permute-start(bf16[1408,512]{1,0:T(8,128)(2,1)} %collective-permute-done), channel_id=1, source_target_pairs={{0,4},{4,8},{8,12},{12,0},{1,5},{5,9},{9,13},{13,1},{2,6},{6,10},{... | collective-permute-start | bytes 4325384 | tf_op jit(solution)/shard_map/ppermute | solution.py:18
  162.5 2.7 constant_dynamic-update-slice_fusion.2
  165.1 0.0 copy-start.1
  165.2 30.1 %collective-permute-done.1 = bf16[1408,512]{1,0:T(8,128)(2,1)} collective-permute-done((bf16[1408,512]{1,0:T(8,128)(2,1)S(1)}, bf16[1408,512]{1,0:T(8,128)(2,1)}, u32[]{:S(2)}, u32[]{:S(2)}) %collective-permute-start.1) | collective-permute-done | bytes 1441824 | tf_op jit(solution)/shard_map/ppermute | solution.py:21
  195.3 2.6 constant_dynamic-update-slice_fusion.1
  197.9 0.0 reduce-scatter.3.cloned.1.call-done
  197.9 0.0 copy-done.1
  197.9 1.1 multiply_reduce_fusion
  199.0 6.1 %psum.7 = f32[192]{0:T(256)S(1)} all-reduce(f32[192]{0:T(256)S(1)} %multiply_reduce_fusion), channel_id=1, replica_groups=mesh['grp'=2,'sp'=4,'tp'=4] {'tp'}, use_global_device_ids=true, to_apply=%region_7.8 | all-reduce | flops 192 | bytes 1536 | tf_op jit(solution)/shard_map/psum | solution.py:101
  205.1 1.0 multiply_convert_fusion
  206.1 8.6 %all_gather.21 = bf16[192,2048]{1,0:T(8,128)(2,1)S(1)} all-gather(bf16[192,512]{1,0:T(8,128)(2,1)S(1)} %multiply_convert_fusion), channel_id=1, replica_groups=mesh['grp'=2,'sp'=4,'tp'=4] {'tp'}, dimensions={1}, use_global_device_ids=true | all-gather | bytes 983040 | tf_op jit(solution)/shard_map/all_gather | solution.py:104
  214.7 16.5 %collective-permute-done.2 = bf16[1408,512]{1,0:T(8,128)(2,1)} collective-permute-done((bf16[1408,512]{1,0:T(8,128)(2,1)}, bf16[1408,512]{1,0:T(8,128)(2,1)}, u32[]{:S(2)}, u32[]{:S(2)}) %collective-permute-start.2) | collective-permute-done | bytes 1441824 | tf_op jit(solution)/shard_map/ppermute | solution.py:18
  231.2 2.6 constant_dynamic-update-slice_fusion
  233.8 7.2 %all-gather.3.cloned.1.call-done = bf16[2048,1408]{1,0:T(8,128)(2,1)} async-done(((bf16[512,1408]{1,0:T(8,128)(2,1)}), bf16[2048,1408]{1,0:T(8,128)(2,1)}) %all-gather.3.cloned.1.call-update) | async-done | bytes 5767184 | tf_op jit(solution)/shard_map/all_gather | solution.py:106
  241.1 5.0 %fusion.36 = f32[192,1408]{1,0:T(8,128)} fusion(bf16[192,2048]{1,0:T(8,128)(2,1)S(1)} %all_gather.21, bf16[2048,1408]{1,0:T(8,128)(2,1)} %all-gather.3.cloned.1.call-done), kind=kOutput, calls=%fused_computation.64 | convolution fusion | flops 1107296256 | bytes 7634944 | tf_op jit(solution)/shard_map/dot_general | solution.py:109
  246.1 0.0 copy-start.2
  246.1 101.7 %all-gather.5.cloned.1.call-done = bf16[2048,1408]{1,0:T(8,128)(2,1)} async-done(((bf16[512,1408]{1,0:T(8,128)(2,1)}), bf16[2048,1408]{1,0:T(8,128)(2,1)}) %all-gather.5.cloned.1.call-update) | async-done | bytes 5767184 | tf_op jit(solution)/shard_map/all_gather | solution.py:107
  347.8 8.2 %convolution_convert_fusion = bf16[192,2048]{1,0:T(8,128)(2,1)} fusion(bf16[1408,2048]{1,0:T(8,128)(2,1)} %constant_dynamic-update-slice_fusion, bf16[192,2048]{1,0:T(8,128)(2,1)S(1)} %all_gather.21, bf16[2048,1408]{1,0:T(8,128)(2,1)} %all-gather.5.cloned.1.call-done, f32[192,1408]{1,0:T(8,128)} %fusion.36), kind=kOutput, calls=%fused_computation.4 | convolution fusion | flops 2216607744 | bytes 14188544 | tf_op jit(solution)/shard_map/dot_general | solution.py:112
  356.0 0.0 reduce-scatter.5.cloned.1.call-update
  356.0 21.6 %reduce-scatter.5.cloned.1.call-done = bf16[192,512]{1,0:T(8,128)(2,1)} async-done(((bf16[192,2048]{1,0:T(8,128)(2,1)}), bf16[192,512]{1,0:T(8,128)(2,1)}) %reduce-scatter.5.cloned.1.call-update) | async-done | bytes 196624 | tf_op jit(solution)/shard_map/reduce_scatter | solution.py:115
  377.6 0.0 copy-done.2
  377.6 1.7 add_convert_fusion
  (6 shorter events, 0.0 us)
Async XLA Ops:
  7.4 49.5 %copy-start = (bf16[2,128,2048]{2,1,0:T(8,128)(2,1)S(1)}, bf16[2,128,2048]{2,1,0:T(8,128)(2,1)}, u32[]{:S(2)}) copy-start(bf16[2,128,2048]{2,1,0:T(8,128)(2,1)} %param.20) | copy-start | bytes 3145732
  7.4 17.0 %copy-start.7 = (bf16[192,128]{1,0:T(8,128)(2,1)S(1)}, bf16[192,128]{1,0:T(8,128)(2,1)}, u32[]{:S(2)}) copy-start(bf16[192,128]{1,0:T(8,128)(2,1)} %param.13) | copy-start | bytes 147460
  7.4 31.5 %copy-start.6 = (bf16[192,128]{1,0:T(8,128)(2,1)S(1)}, bf16[192,128]{1,0:T(8,128)(2,1)}, u32[]{:S(2)}) copy-start(bf16[192,128]{1,0:T(8,128)(2,1)} %param.12) | copy-start | bytes 147460
  7.4 31.7 %copy-start.5 = (bf16[192,2,128]{2,1,0:T(2,128)(2,1)S(1)}, bf16[192,2,128]{2,1,0:T(2,128)(2,1)}, u32[]{:S(2)}) copy-start(bf16[192,2,128]{2,1,0:T(2,128)(2,1)} %param.16) | copy-start | bytes 294916
  7.4 190.5 %reduce-scatter.3.cloned.1.call-start = ((), (), s32[]{:S(2)}) async-start(), calls=%async_computation.2 | async-start | bytes 983040 | tf_op jit(solution)/shard_map/reduce_scatter | solution.py:97
  24.2 29.6 %copy-start.4 = (bf16[192,256]{1,0:T(8,128)(2,1)S(1)}, bf16[192,256]{1,0:T(8,128)(2,1)}, u32[]{:S(2)}) copy-start(bf16[192,256]{1,0:T(8,128)(2,1)} %param.14) | copy-start | bytes 294916
  55.9 0.7 copy-start.8
  58.2 1.4 copy-start.3
  58.2 5.4 %copy-start.9 = (bf16[512]{0:T(512)(128)(2,1)S(1)}, bf16[512]{0:T(512)(128)(2,1)}, u32[]{:S(2)}) copy-start(bf16[512]{0:T(512)(128)(2,1)} %param.19) | copy-start | bytes 3076
  58.2 182.9 %all-gather.3.cloned.1.call-start = ((), (), s32[]{:S(2)}) async-start(), calls=%async_computation.3 | async-start | bytes 7208960 | tf_op jit(solution)/shard_map/all_gather | solution.py:106
  58.8 289.0 %all-gather.5.cloned.1.call-start = ((), (), s32[]{:S(2)}) async-start(), calls=%async_computation.4 | async-start | bytes 7208960 | tf_op jit(solution)/shard_map/all_gather | solution.py:107
  59.4 318.2 %reduce-scatter.5.cloned.1.call-start = ((), (), s32[]{:S(2)}) async-start(), calls=%async_computation.5 | async-start | bytes 983040 | tf_op jit(solution)/shard_map/reduce_scatter | solution.py:115
  59.6 57.4 %collective-permute-start = (bf16[1408,512]{1,0:T(8,128)(2,1)S(1)}, bf16[1408,512]{1,0:T(8,128)(2,1)}, u32[]{:S(2)}, u32[]{:S(2)}) collective-permute-start(bf16[1408,512]{1,0:T(8,128)(2,1)S(1)} %copy-done.3), channel_id=1, source_target_pairs={{0,4},{4,8},{8,12},{12,0},{1,5},{5,9},{9,13},{13,1},{2,6},{6,10},{... | collective-permute-start | bytes 4325384 | tf_op jit(solution)/shard_map/ppermute | solution.py:18
  61.5 133.8 %collective-permute-start.1 = (bf16[1408,512]{1,0:T(8,128)(2,1)S(1)}, bf16[1408,512]{1,0:T(8,128)(2,1)}, u32[]{:S(2)}, u32[]{:S(2)}) collective-permute-start(bf16[1408,512]{1,0:T(8,128)(2,1)S(1)} %copy-done.3), channel_id=1, source_target_pairs={{0,12},{4,0},{8,4},{12,8},{1,13},{5,1},{9,5},{13,9},{2,14},{6,2},{... | collective-permute-start | bytes 4325384 | tf_op jit(solution)/shard_map/ppermute | solution.py:21
  117.0 114.3 %collective-permute-start.2 = (bf16[1408,512]{1,0:T(8,128)(2,1)}, bf16[1408,512]{1,0:T(8,128)(2,1)}, u32[]{:S(2)}, u32[]{:S(2)}) collective-permute-start(bf16[1408,512]{1,0:T(8,128)(2,1)} %collective-permute-done), channel_id=1, source_target_pairs={{0,4},{4,8},{8,12},{12,0},{1,5},{5,9},{9,13},{13,1},{2,6},{6,10},{... | collective-permute-start | bytes 4325384 | tf_op jit(solution)/shard_map/ppermute | solution.py:18
  165.1 32.8 %copy-start.1 = (bf16[192,512]{1,0:T(8,128)(2,1)S(1)}, bf16[192,512]{1,0:T(8,128)(2,1)}, u32[]{:S(2)}) copy-start(bf16[192,512]{1,0:T(8,128)(2,1)} %param.18) | copy-start | bytes 589828
  246.1 131.5 %copy-start.2 = (bf16[192,512]{1,0:T(8,128)(2,1)S(1)}, bf16[192,512]{1,0:T(8,128)(2,1)}, u32[]{:S(2)}) copy-start(bf16[192,512]{1,0:T(8,128)(2,1)} %reduce-scatter.3.cloned.1.call-done) | copy-start | bytes 589828
Sparse Core Ops, SparseCore 0:
  58.3 24.8 reduce-scatter.2
  356.1 21.4 reduce-scatter.4
Sparse Core Ops, SparseCore 1:
  60.3 180.8 all-gather.2
  242.5 105.2 all-gather.4
